TPU v7x, 32 devices: a whole 2x2x4 slice. The times are simulated.
32 devices in a mesh: fs: 16 (over z, y, x), tp: 2 (over core).
Axes of the slice: x: 2, y: 2, z: 4, core: 2. Of those that a mesh axis runs over, the one named last changes fastest.
Arguments:
- late_input: bfloat16 [2048, 2048], P('fs', 'tp'), may hold values from -6 to 6
- up_weight: bfloat16 [2048, 4096], P('tp', 'fs'), may hold values from -0.125 to 0.125
- down_weight: bfloat16 [4096, 2048], P('fs', 'tp'), may hold values from -0.09375 to 0.09375
- early_input: bfloat16 [2048, 2048], P('fs', 'tp'), may hold values from -6 to 6
- early_pre: bfloat16 [2048, 4096], P('fs'), may hold values from -6 to 6
- cotangent: bfloat16 [2048, 2048], P('fs', 'tp'), may hold values from -6 to 6
- up_sum: float32 [2048, 4096], P('tp', 'fs'), may hold values from -24 to 24
- down_sum: float32 [4096, 2048], P('fs', 'tp'), may hold values from -24 to 24
Outputs:
- late_pre: bfloat16 [2048, 4096], P('fs')
- late_out: bfloat16 [2048, 2048], P('fs', 'tp')
- input_grad: bfloat16 [2048, 2048], P('fs', 'tp')
- up_total: float32 [2048, 4096], P('tp', 'fs')
- down_total: float32 [4096, 2048], P('fs', 'tp')
All inputs are finite; a program needn't handle non-finite values.
Results may differ from a plain program's by a relative error of at most 0.025.
Values may be sent and summed in bfloat16 or wider, within the bound.
A program may use at most 128 MiB of HBM per device.

v0:
```python
import jax
import jax.numpy as jnp
from jax import lax
from jax.sharding import PartitionSpec as P


def contract_rows(left, right):
    return lax.dot_general(
        left, right, (((0,), (0,)), ((), ())), preferred_element_type=jnp.float32
    )


def contract_cols(left, right):
    return lax.dot_general(
        left, right, (((1,), (1,)), ((), ())), preferred_element_type=jnp.float32
    )


def body(late_input, up_weight, down_weight, early_input, early_pre, cotangent, up_sum, down_sum):
    up_gathered = lax.all_gather(up_weight, "fs", axis=1, tiled=True)
    down_gathered = lax.all_gather(down_weight, "fs", axis=0, tiled=True)
    pre_terms = jnp.dot(late_input, up_gathered, preferred_element_type=jnp.float32)
    pre_summed = lax.psum(pre_terms.astype(jnp.bfloat16), "tp")
    late_hidden = jnp.square(jax.nn.relu(pre_summed.astype(jnp.float32))).astype(jnp.bfloat16)
    early_float = early_pre.astype(jnp.float32)
    early_hidden = jnp.square(jax.nn.relu(early_float)).astype(jnp.bfloat16)
    late_out = jnp.dot(late_hidden, down_gathered, preferred_element_type=jnp.float32).astype(
        jnp.bfloat16
    )
    grad_terms = contract_cols(cotangent, down_gathered)
    hidden_grad = lax.psum(grad_terms.astype(jnp.bfloat16), "tp").astype(jnp.float32)
    pre_grad = (hidden_grad * 2.0 * jax.nn.relu(early_float)).astype(jnp.bfloat16)
    input_grad = contract_cols(pre_grad, up_gathered).astype(jnp.bfloat16)
    grad_local, hidden_local = (
        lax.all_to_all(pre_grad, "fs", split_axis=1, concat_axis=0, tiled=True),
        lax.all_to_all(early_hidden, "fs", split_axis=1, concat_axis=0, tiled=True),
    )
    rows = grad_local
    up_grad = contract_rows(lax.all_gather(early_input, "fs", axis=0, tiled=True), rows)
    up_total = up_sum + up_grad
    rows = hidden_local
    down_grad = contract_rows(rows, lax.all_gather(cotangent, "fs", axis=0, tiled=True))
    down_total = down_sum + down_grad
    return (pre_summed, late_out, input_grad, up_total, down_total)


def solution(mesh):
    in_specs = (
        P("fs", "tp"),
        P("tp", "fs"),
        P("fs", "tp"),
        P("fs", "tp"),
        P("fs", None),
        P("fs", "tp"),
        P("tp", "fs"),
        P("fs", "tp"),
    )
    out_specs = (P("fs", None), P("fs", "tp"), P("fs", "tp"), P("tp", "fs"), P("fs", "tp"))
    return jax.shard_map(body, mesh=mesh, in_specs=in_specs, out_specs=out_specs, check_vma=False)
```

profile of v0, /device:TPU:0, one launch (start us, length us, event | category | flops | bytes accessed | tf_op | source)
XLA Modules:
  0.0 475.7 jit_solution(18036895991787188094)
XLA Ops:
  7.2 0.0 copy-start
  7.2 0.0 all-gather.7.cloned.1.call-start
  7.2 0.7 all-gather.7.cloned.1.call-update
  7.9 0.0 all-gather.5.cloned.1.call-start
  8.0 0.7 all-gather.5.cloned.1.call-update
  8.7 0.0 all-reduce.3.cloned.1.call-start
  8.7 117.1 %all-gather.7.cloned.1.call-done = bf16[4096,1024]{1,0:T(8,128)(2,1)} async-done(((bf16[256,1024]{1,0:T(8,128)(2,1)}), bf16[4096,1024]{1,0:T(8,128)(2,1)}) %all-gather.7.cloned.1.call-update) | async-done | bytes 8388624 | tf_op jit(solution)/shard_map/all_gather | solution.py:21
  125.8 7.3 %convolution_convert_fusion = bf16[128,4096]{1,0:T(8,128)(2,1)} fusion(bf16[128,1024]{1,0:T(8,128)(2,1)} %param.13, bf16[4096,1024]{1,0:T(8,128)(2,1)} %all-gather.7.cloned.1.call-done), kind=kOutput, calls=%fused_computation | convolution fusion | flops 1074266112 | bytes 9699328 | tf_op jit(solution)/shard_map/dot_general | solution.py:14
  133.2 0.0 copy-start.4
  133.2 128.1 %all-gather.5.cloned.1.call-done = bf16[1024,4096]{1,0:T(8,128)(2,1)} async-done(((bf16[1024,256]{1,0:T(8,128)(2,1)}), bf16[1024,4096]{1,0:T(8,128)(2,1)}) %all-gather.5.cloned.1.call-update) | async-done | bytes 8388624 | tf_op jit(solution)/shard_map/all_gather | solution.py:20
  261.2 0.0 copy-done
  261.2 5.6 %convolution_convert_fusion.1 = bf16[128,4096]{1,0:T(8,128)(2,1)} fusion(bf16[128,1024]{1,0:T(8,128)(2,1)S(1)} %copy-done, bf16[1024,4096]{1,0:T(8,128)(2,1)} %all-gather.5.cloned.1.call-done), kind=kOutput, calls=%fused_computation.1 | convolution fusion | flops 1074266112 | bytes 9699328 | tf_op jit(solution)/shard_map/dot_general | solution.py:22
  266.8 0.0 all-reduce.3.cloned.1.call-update
  266.9 0.0 all-gather.9.cloned.1.call-start
  266.9 0.5 all-gather.9.cloned.1.call-update
  267.4 0.0 all-gather.11.cloned.1.call-start
  267.5 0.5 all-gather.11.cloned.1.call-update
  268.0 18.6 %all-reduce.3.cloned.1.call-done = (bf16[128,4096]{1,0:T(8,128)(2,1)}, bf16[128,4096]{1,0:T(8,128)(2,1)}) async-done(((bf16[128,4096]{1,0:T(8,128)(2,1)}, bf16[128,4096]{1,0:T(8,128)(2,1)}), (bf16[128,4096]{1,0:T(8,128)(2,1)}, bf16[128,4096]{1,0:T(8,128)(2,1)})) %all-reduce.3.cloned.1.call-update) | async-done | bytes 2097168 | tf_op jit(solution)/shard_map/psum | solution.py:23
  286.6 0.0 copy-done.4
  286.6 1.7 multiply_convert_fusion
  288.3 0.0 copy-start.1
  288.4 1.1 copy.24
  289.4 6.8 %all-to-all-start = ((bf16[128,16,256]{2,0,1:T(8,128)(2,1)}), bf16[128,16,256]{2,0,1:T(8,128)(2,1)}, u32[]{:S(2)}, u32[]{:S(2)}) async-start(bf16[128,16,256]{2,0,1:T(8,128)(2,1)} %bitcast.28), calls=%async_computation | async-start | bytes 2097152 | tf_op jit(solution)/shard_map/all_to_all | solution.py:35
  296.3 1.1 copy.23
  297.4 29.2 %all-to-all-done = bf16[128,16,256]{2,0,1:T(8,128)(2,1)} async-done(((bf16[128,16,256]{2,0,1:T(8,128)(2,1)}), bf16[128,16,256]{2,0,1:T(8,128)(2,1)}, u32[]{:S(2)}, u32[]{:S(2)}) %all-to-all-start) | async-done | bytes 1048608 | tf_op jit(solution)/shard_map/all_to_all | solution.py:35
  326.6 6.5 %all-to-all-start.1 = ((bf16[128,16,256]{2,0,1:T(8,128)(2,1)}), bf16[128,16,256]{2,0,1:T(8,128)(2,1)}, u32[]{:S(2)}, u32[]{:S(2)}) async-start(bf16[128,16,256]{2,0,1:T(8,128)(2,1)} %bitcast.27), calls=%async_computation.1 | async-start | bytes 2097152 | tf_op jit(solution)/shard_map/all_to_all | solution.py:36
  333.1 0.0 copy-done.1
  333.1 1.3 copy.16
  334.5 0.0 copy-start.2
  334.5 7.1 %convolution_convert_fusion.2 = bf16[128,1024]{1,0:T(8,128)(2,1)} fusion(bf16[128,4096]{1,0:T(8,128)(2,1)S(1)} %get-tuple-element.18, bf16[1024,4096]{1,0:T(8,128)(2,1)} %all-gather.5.cloned.1.call-done), kind=kOutput, calls=%fused_computation.9 | convolution fusion | flops 1073872896 | bytes 9699328 | tf_op jit(solution)/shard_map/dot_general | solution.py:14
  341.5 0.0 copy-done.2
  341.5 0.0 copy-start.3
  341.5 5.4 %convolution_convert_fusion.3 = bf16[128,1024]{1,0:T(8,128)(2,1)} fusion(bf16[4096,1024]{1,0:T(8,128)(2,1)} %all-gather.7.cloned.1.call-done, bf16[128,4096]{1,0:T(8,128)(2,1)S(1)} %copy-done.2), kind=kOutput, calls=%fused_computation.10 | convolution fusion | flops 1075970048 | bytes 9699328 | tf_op jit(solution)/shard_map/dot_general | solution.py:27
  347.0 39.4 %all-gather.9.cloned.1.call-done = bf16[2048,1024]{1,0:T(8,128)(2,1)} async-done(((bf16[128,1024]{1,0:T(8,128)(2,1)}), bf16[2048,1024]{1,0:T(8,128)(2,1)}) %all-gather.9.cloned.1.call-update) | async-done | bytes 4194320 | tf_op jit(solution)/shard_map/all_gather | solution.py:39
  386.4 0.0 copy-done.3
  386.4 3.8 fusion
  390.2 1.3 copy.18
  391.5 71.7 %all-gather.11.cloned.1.call-done = bf16[2048,1024]{1,0:T(8,128)(2,1)} async-done(((bf16[128,1024]{1,0:T(8,128)(2,1)}), bf16[2048,1024]{1,0:T(8,128)(2,1)}) %all-gather.11.cloned.1.call-update) | async-done | bytes 4194320 | tf_op jit(solution)/shard_map/all_gather | solution.py:42
  463.2 0.0 all-to-all-done.1
  463.2 5.0 %convolution_add_fusion = f32[256,1024]{1,0:T(8,128)} fusion(f32[256,1024]{1,0:T(8,128)} %param.15, bf16[2048,256]{1,0:T(8,128)(2,1)} %bitcast.4, bf16[2048,1024]{1,0:T(8,128)(2,1)} %all-gather.11.cloned.1.call-done), kind=kOutput, calls=%fused_computation.8 | convolution fusion | flops 1074003968 | bytes 7340032 | tf_op jit(solution)/shard_map/dot_general | solution.py:8
  468.2 1.0 copy.27
Async XLA Ops:
  7.2 254.1 %copy-start = (bf16[128,1024]{1,0:T(8,128)(2,1)S(1)}, bf16[128,1024]{1,0:T(8,128)(2,1)}, u32[]{:S(2)}) copy-start(bf16[128,1024]{1,0:T(8,128)(2,1)} %param.8) | copy-start | bytes 786436
  7.2 118.6 %all-gather.7.cloned.1.call-start = ((), (), s32[]{:S(2)}) async-start(), calls=%async_computation.3 | async-start | bytes 8912896 | tf_op jit(solution)/shard_map/all_gather | solution.py:21
  7.9 253.3 %all-gather.5.cloned.1.call-start = ((), (), s32[]{:S(2)}) async-start(), calls=%async_computation.2 | async-start | bytes 8912896 | tf_op jit(solution)/shard_map/all_gather | solution.py:20
  8.7 277.9 %all-reduce.3.cloned.1.call-start = ((), (), s32[]{:S(2)}) async-start(), calls=%async_computation.6 | async-start | bytes 4194304 | tf_op jit(solution)/shard_map/psum | solution.py:23
  133.2 153.5 %copy-start.4 = (bf16[128,4096]{1,0:T(8,128)(2,1)S(1)}, bf16[128,4096]{1,0:T(8,128)(2,1)}, u32[]{:S(2)}) copy-start(bf16[128,4096]{1,0:T(8,128)(2,1)} %param.12) | copy-start | bytes 3145732
  266.9 119.5 %all-gather.9.cloned.1.call-start = ((), (), s32[]{:S(2)}) async-start(), calls=%async_computation.4 | async-start | bytes 4456448 | tf_op jit(solution)/shard_map/all_gather | solution.py:39
  267.4 195.7 %all-gather.11.cloned.1.call-start = ((), (), s32[]{:S(2)}) async-start(), calls=%async_computation.5 | async-start | bytes 4456448 | tf_op jit(solution)/shard_map/all_gather | solution.py:42
  288.3 44.8 %copy-start.1 = (f32[1024,256]{1,0:T(8,128)S(1)}, f32[1024,256]{1,0:T(8,128)}, u32[]{:S(2)}) copy-start(f32[1024,256]{1,0:T(8,128)} %param.14) | copy-start | bytes 3145732
  289.4 37.2 %all-to-all-start = ((bf16[128,16,256]{2,0,1:T(8,128)(2,1)}), bf16[128,16,256]{2,0,1:T(8,128)(2,1)}, u32[]{:S(2)}, u32[]{:S(2)}) async-start(bf16[128,16,256]{2,0,1:T(8,128)(2,1)} %bitcast.28), calls=%async_computation | async-start | bytes 2097152 | tf_op jit(solution)/shard_map/all_to_all | solution.py:35
  326.6 136.6 %all-to-all-start.1 = ((bf16[128,16,256]{2,0,1:T(8,128)(2,1)}), bf16[128,16,256]{2,0,1:T(8,128)(2,1)}, u32[]{:S(2)}, u32[]{:S(2)}) async-start(bf16[128,16,256]{2,0,1:T(8,128)(2,1)} %bitcast.27), calls=%async_computation.1 | async-start | bytes 2097152 | tf_op jit(solution)/shard_map/all_to_all | solution.py:36
  334.5 7.1 %copy-start.2 = (bf16[128,4096]{1,0:T(8,128)(2,1)S(1)}, bf16[128,4096]{1,0:T(8,128)(2,1)}, u32[]{:S(2)}) copy-start(bf16[128,4096]{1,0:T(8,128)(2,1)} %get-tuple-element.19) | copy-start | bytes 3145732
  341.5 44.8 %copy-start.3 = (f32[1024,256]{0,1:T(8,128)S(1)}, f32[1024,256]{0,1:T(8,128)}, u32[]{:S(2)}) copy-start(f32[1024,256]{0,1:T(8,128)} %copy.16) | copy-start | bytes 3145732
Sparse Core Ops, SparseCore 0:
  10.8 115.0 all-gather.6
  128.5 132.6 all-gather.4
  267.0 19.5 all-reduce.2
  289.2 97.1 all-gather.8
  389.0 74.1 all-gather.10
where the time goes:
time: 476 us
  waiting for transfers between devices  407 us (86%)
  matrix products  34.3 us (7%)
  between operations  13.8 us (3%)
  starting transfers between devices  13.6 us (3%)
  local copies, waits for them, and re-layouts  5.76 us (1%)
    all_gather x1, waiting for transfers between devices, body(): up_gathered = lax.all_gather(up_weight, 'fs', axis=1, tiled=True)  128 us
    all_gather x1, waiting for transfers between devices, body(): down_gathered = lax.all_gather(down_weight, 'fs', axis=0, tiled=True)  117 us
    all_gather x1, waiting for transfers between devices, body(): lax.all_gather(cotangent, 'fs', axis=0, tiled=True)  71.7 us
    all_gather x1, waiting for transfers between devices, body(): lax.all_gather(early_input, 'fs', axis=0, tiled=True)  39.4 us
    all_to_all x1, waiting for transfers between devices, body(): lax.all_to_all(pre_grad, 'fs', split_axis=1, concat_axis=0, tiled=True)  29.2 us
    psum x1, waiting for transfers between devices, body(): pre_summed = lax.psum(pre_terms.astype(jnp.bfloat16), 'tp')  18.6 us
    dot_general x2, matrix products, contract_cols(): lax.dot_general(left, right, (((1,), (1,)), ((), ())), preferred_element_...  14.4 us
  transfers between devices with their start and end apart: 7, of which 6 were waited for; matrix products, arithmetic and copies ran while one was open for 6% of the time, Pallas kernels for 0%

commit v1 on v0

--- a/solution.py
+++ b/solution.py
@@ -17,7 +17,8 @@
 
 
 def body(late_input, up_weight, down_weight, early_input, early_pre, cotangent, up_sum, down_sum):
-    up_gathered = lax.all_gather(up_weight, "fs", axis=1, tiled=True)
+    terms = lax.all_gather(up_weight, "fs", axis=0, tiled=False)
+    up_gathered = jnp.concatenate(terms, axis=1)
     down_gathered = lax.all_gather(down_weight, "fs", axis=0, tiled=True)
     pre_terms = jnp.dot(late_input, up_gathered, preferred_element_type=jnp.float32)
     pre_summed = lax.psum(pre_terms.astype(jnp.bfloat16), "tp")

time: 476 us -> 456 us (0.958)
  waiting for transfers between devices: 407 us -> 374 us
  local copies, waits for them, and re-layouts: 5.76 us -> 18.1 us
    all_gather x1, waiting for transfers between devices: 117 us -> 93.7 us  [body(): down_gathered = lax.all_gather(down_weight, 'fs', axis=0, tiled=True)]
    reshape x0 -> x1, local copies, waits for them, and re-layouts: none -> 12.3 us  [body(): up_gathered = jnp.concatenate(terms, axis=1)]
    all_gather x1, waiting for transfers between devices: 128 us -> 117 us  [body(): terms = lax.all_gather(up_weight, 'fs', axis=0, tiled=False)]
  transfers between devices with their start and end apart: 7 -> 7, of which waited for: 6 -> 6; matrix products, arithmetic and copies ran while one was open for 6% -> 9% of each run, Pallas kernels for 0% -> 0%
where the time goes in v1:
time: 456 us; the launch traced here: 455 us
  waiting for transfers between devices  374 us (82%)
  matrix products  34.3 us (8%)
  local copies, waits for them, and re-layouts  18.1 us (4%)
  between operations  13.8 us (3%)
  starting transfers between devices  13.6 us (3%)
    all_gather x1, waiting for transfers between devices, body(): terms = lax.all_gather(up_weight, 'fs', axis=0, tiled=False)  117 us
    all_gather x1, waiting for transfers between devices, body(): down_gathered = lax.all_gather(down_weight, 'fs', axis=0, tiled=True)  93.7 us
    all_gather x1, waiting for transfers between devices, body(): lax.all_gather(cotangent, 'fs', axis=0, tiled=True)  71.7 us
    all_gather x1, waiting for transfers between devices, body(): lax.all_gather(early_input, 'fs', axis=0, tiled=True)  41 us
    all_to_all x1, waiting for transfers between devices, body(): lax.all_to_all(pre_grad, 'fs', split_axis=1, concat_axis=0, tiled=True)  29.2 us
    psum x1, waiting for transfers between devices, body(): pre_summed = lax.psum(pre_terms.astype(jnp.bfloat16), 'tp')  18.5 us
    dot_general x2, matrix products, contract_cols(): lax.dot_general(left, right, (((1,), (1,)), ((), ())), preferred_element_...  12.7 us
    reshape x1, local copies, waits for them, and re-layouts, body(): up_gathered = jnp.concatenate(terms, axis=1)  12.3 us
  transfers between devices with their start and end apart: 7, of which 6 were waited for; matrix products, arithmetic and copies ran while one was open for 9% of the time, Pallas kernels for 0%

profile of v1, /device:TPU:0, one launch (start us, length us, event | category | flops | bytes accessed | tf_op | source)
XLA Modules:
  0.0 455.2 jit_solution(17397854329710446833)
XLA Ops:
  7.2 0.0 copy-start
  7.2 0.0 all-gather.12.cloned.1.call-start
  7.2 0.7 all-gather.12.cloned.1.call-update
  7.9 0.0 all-gather.6.cloned.1.call-start
  8.0 0.7 all-gather.6.cloned.1.call-update
  8.7 0.0 all-reduce.3.cloned.1.call-start
  8.7 117.1 %all-gather.12.cloned.1.call-done = bf16[16384,256]{1,0:T(8,128)(2,1)} async-done(((bf16[1024,256]{1,0:T(8,128)(2,1)}), bf16[16384,256]{1,0:T(8,128)(2,1)}) %all-gather.12.cloned.1.call-update) | async-done | bytes 8388624 | tf_op jit(solution)/shard_map/all_gather | solution.py:20
  125.8 12.3 %copy.19 = bf16[1024,16,256]{0,2,1:T(8,128)(2,1)} copy(bf16[1024,16,256]{2,0,1:T(8,128)(2,1)} %bitcast.36) | data formatting | bytes 16777216 | tf_op jit(solution)/shard_map/reshape | solution.py:21
  138.1 0.0 copy-done
  138.1 0.0 copy-start.1
  138.1 7.3 %convolution_convert_fusion.1 = bf16[128,4096]{1,0:T(8,128)(2,1)} fusion(bf16[128,1024]{1,0:T(8,128)(2,1)S(1)} %copy-done, bf16[1024,4096]{0,1:T(8,128)(2,1)} %bitcast.33), kind=kOutput, calls=%fused_computation.1 | convolution fusion | flops 1074266112 | bytes 9699328 | tf_op jit(solution)/shard_map/dot_general | solution.py:23
  145.4 0.0 copy-start.5
  145.4 93.7 %all-gather.6.cloned.1.call-done = bf16[4096,1024]{1,0:T(8,128)(2,1)} async-done(((bf16[256,1024]{1,0:T(8,128)(2,1)}), bf16[4096,1024]{1,0:T(8,128)(2,1)}) %all-gather.6.cloned.1.call-update) | async-done | bytes 8388624 | tf_op jit(solution)/shard_map/all_gather | solution.py:22
  239.1 0.0 copy-done.1
  239.1 7.2 %convolution_convert_fusion = bf16[128,4096]{1,0:T(8,128)(2,1)} fusion(bf16[128,1024]{1,0:T(8,128)(2,1)S(1)} %copy-done.1, bf16[4096,1024]{1,0:T(8,128)(2,1)} %all-gather.6.cloned.1.call-done), kind=kOutput, calls=%fused_computation | convolution fusion | flops 1074266112 | bytes 9699328 | tf_op jit(solution)/shard_map/dot_general | solution.py:14
  246.3 0.0 all-reduce.3.cloned.1.call-update
  246.3 0.0 all-gather.8.cloned.1.call-start
  246.4 0.5 all-gather.8.cloned.1.call-update
  246.9 0.0 all-gather.10.cloned.1.call-start
  247.0 0.5 all-gather.10.cloned.1.call-update
  247.5 18.5 %all-reduce.3.cloned.1.call-done = (bf16[128,4096]{1,0:T(8,128)(2,1)}, bf16[128,4096]{1,0:T(8,128)(2,1)}) async-done(((bf16[128,4096]{1,0:T(8,128)(2,1)}, bf16[128,4096]{1,0:T(8,128)(2,1)}), (bf16[128,4096]{1,0:T(8,128)(2,1)}, bf16[128,4096]{1,0:T(8,128)(2,1)})) %all-reduce.3.cloned.1.call-update) | async-done | bytes 2097168 | tf_op jit(solution)/shard_map/psum | solution.py:24
  266.1 0.0 copy-done.5
  266.1 1.7 multiply_convert_fusion
  267.8 0.0 copy-start.2
  267.8 1.1 copy.29
  268.9 6.8 %all-to-all-start = ((bf16[128,16,256]{2,0,1:T(8,128)(2,1)}), bf16[128,16,256]{2,0,1:T(8,128)(2,1)}, u32[]{:S(2)}, u32[]{:S(2)}) async-start(bf16[128,16,256]{2,0,1:T(8,128)(2,1)} %bitcast.32), calls=%async_computation | async-start | bytes 2097152 | tf_op jit(solution)/shard_map/all_to_all | solution.py:36
  275.7 1.1 copy.28
  276.8 29.2 %all-to-all-done = bf16[128,16,256]{2,0,1:T(8,128)(2,1)} async-done(((bf16[128,16,256]{2,0,1:T(8,128)(2,1)}), bf16[128,16,256]{2,0,1:T(8,128)(2,1)}, u32[]{:S(2)}, u32[]{:S(2)}) %all-to-all-start) | async-done | bytes 1048608 | tf_op jit(solution)/shard_map/all_to_all | solution.py:36
  306.1 6.5 %all-to-all-start.1 = ((bf16[128,16,256]{2,0,1:T(8,128)(2,1)}), bf16[128,16,256]{2,0,1:T(8,128)(2,1)}, u32[]{:S(2)}, u32[]{:S(2)}) async-start(bf16[128,16,256]{2,0,1:T(8,128)(2,1)} %bitcast.31), calls=%async_computation.1 | async-start | bytes 2097152 | tf_op jit(solution)/shard_map/all_to_all | solution.py:37
  312.6 0.0 copy-done.2
  312.6 1.3 copy.21
  313.9 0.0 copy-start.3
  313.9 5.5 %convolution_convert_fusion.2 = bf16[128,1024]{1,0:T(8,128)(2,1)} fusion(bf16[128,4096]{1,0:T(8,128)(2,1)S(1)} %get-tuple-element.23, bf16[1024,4096]{0,1:T(8,128)(2,1)} %bitcast.34), kind=kOutput, calls=%fused_computation.9 | convolution fusion | flops 1073872896 | bytes 9699328 | tf_op jit(solution)/shard_map/dot_general | solution.py:14
  319.4 0.0 copy-done.3
  319.4 0.0 copy-start.4
  319.4 5.4 %convolution_convert_fusion.3 = bf16[128,1024]{1,0:T(8,128)(2,1)} fusion(bf16[4096,1024]{1,0:T(8,128)(2,1)} %all-gather.6.cloned.1.call-done, bf16[128,4096]{1,0:T(8,128)(2,1)S(1)} %copy-done.3), kind=kOutput, calls=%fused_computation.10 | convolution fusion | flops 1075970048 | bytes 9699328 | tf_op jit(solution)/shard_map/dot_general | solution.py:28
  324.8 41.0 %all-gather.8.cloned.1.call-done = bf16[2048,1024]{1,0:T(8,128)(2,1)} async-done(((bf16[128,1024]{1,0:T(8,128)(2,1)}), bf16[2048,1024]{1,0:T(8,128)(2,1)}) %all-gather.8.cloned.1.call-update) | async-done | bytes 4194320 | tf_op jit(solution)/shard_map/all_gather | solution.py:40
  365.8 0.0 copy-done.4
  365.8 3.8 fusion
  369.6 1.3 copy.23
  370.9 71.7 %all-gather.10.cloned.1.call-done = bf16[2048,1024]{1,0:T(8,128)(2,1)} async-done(((bf16[128,1024]{1,0:T(8,128)(2,1)}), bf16[2048,1024]{1,0:T(8,128)(2,1)}) %all-gather.10.cloned.1.call-update) | async-done | bytes 4194320 | tf_op jit(solution)/shard_map/all_gather | solution.py:43
  442.6 0.0 all-to-all-done.1
  442.6 5.0 %convolution_add_fusion = f32[256,1024]{1,0:T(8,128)} fusion(f32[256,1024]{1,0:T(8,128)} %param.15, bf16[2048,256]{1,0:T(8,128)(2,1)} %bitcast.7, bf16[2048,1024]{1,0:T(8,128)(2,1)} %all-gather.10.cloned.1.call-done), kind=kOutput, calls=%fused_computation.8 | convolution fusion | flops 1074003968 | bytes 7340032 | tf_op jit(solution)/shard_map/dot_general | solution.py:8
  447.7 1.0 copy.32
Async XLA Ops:
  7.2 131.0 %copy-start = (bf16[128,1024]{1,0:T(8,128)(2,1)S(1)}, bf16[128,1024]{1,0:T(8,128)(2,1)}, u32[]{:S(2)}) copy-start(bf16[128,1024]{1,0:T(8,128)(2,1)} %param.8) | copy-start | bytes 786436
  7.2 118.6 %all-gather.12.cloned.1.call-start = ((), (), s32[]{:S(2)}) async-start(), calls=%async_computation.5 | async-start | bytes 8912896 | tf_op jit(solution)/shard_map/all_gather | solution.py:20
  7.9 231.2 %all-gather.6.cloned.1.call-start = ((), (), s32[]{:S(2)}) async-start(), calls=%async_computation.2 | async-start | bytes 8912896 | tf_op jit(solution)/shard_map/all_gather | solution.py:22
  8.7 257.4 %all-reduce.3.cloned.1.call-start = ((), (), s32[]{:S(2)}) async-start(), calls=%async_computation.6 | async-start | bytes 4194304 | tf_op jit(solution)/shard_map/psum | solution.py:24
  138.1 101.0 %copy-start.1 = (bf16[128,1024]{1,0:T(8,128)(2,1)S(1)}, bf16[128,1024]{1,0:T(8,128)(2,1)}, u32[]{:S(2)}) copy-start(bf16[128,1024]{1,0:T(8,128)(2,1)} %param.13) | copy-start | bytes 786436
  145.4 120.6 %copy-start.5 = (bf16[128,4096]{1,0:T(8,128)(2,1)S(1)}, bf16[128,4096]{1,0:T(8,128)(2,1)}, u32[]{:S(2)}) copy-start(bf16[128,4096]{1,0:T(8,128)(2,1)} %param.12) | copy-start | bytes 3145732
  246.3 119.5 %all-gather.8.cloned.1.call-start = ((), (), s32[]{:S(2)}) async-start(), calls=%async_computation.3 | async-start | bytes 4456448 | tf_op jit(solution)/shard_map/all_gather | solution.py:40
  246.9 195.7 %all-gather.10.cloned.1.call-start = ((), (), s32[]{:S(2)}) async-start(), calls=%async_computation.4 | async-start | bytes 4456448 | tf_op jit(solution)/shard_map/all_gather | solution.py:43
  267.8 44.8 %copy-start.2 = (f32[1024,256]{1,0:T(8,128)S(1)}, f32[1024,256]{1,0:T(8,128)}, u32[]{:S(2)}) copy-start(f32[1024,256]{1,0:T(8,128)} %param.14) | copy-start | bytes 3145732
  268.9 37.2 %all-to-all-start = ((bf16[128,16,256]{2,0,1:T(8,128)(2,1)}), bf16[128,16,256]{2,0,1:T(8,128)(2,1)}, u32[]{:S(2)}, u32[]{:S(2)}) async-start(bf16[128,16,256]{2,0,1:T(8,128)(2,1)} %bitcast.32), calls=%async_computation | async-start | bytes 2097152 | tf_op jit(solution)/shard_map/all_to_all | solution.py:36
  306.1 136.6 %all-to-all-start.1 = ((bf16[128,16,256]{2,0,1:T(8,128)(2,1)}), bf16[128,16,256]{2,0,1:T(8,128)(2,1)}, u32[]{:S(2)}, u32[]{:S(2)}) async-start(bf16[128,16,256]{2,0,1:T(8,128)(2,1)} %bitcast.31), calls=%async_computation.1 | async-start | bytes 2097152 | tf_op jit(solution)/shard_map/all_to_all | solution.py:37
  313.9 5.5 %copy-start.3 = (bf16[128,4096]{1,0:T(8,128)(2,1)S(1)}, bf16[128,4096]{1,0:T(8,128)(2,1)}, u32[]{:S(2)}) copy-start(bf16[128,4096]{1,0:T(8,128)(2,1)} %get-tuple-element.24) | copy-start | bytes 3145732
  319.4 46.5 %copy-start.4 = (f32[1024,256]{0,1:T(8,128)S(1)}, f32[1024,256]{0,1:T(8,128)}, u32[]{:S(2)}) copy-start(f32[1024,256]{0,1:T(8,128)} %copy.21) | copy-start | bytes 3145732
Sparse Core Ops, SparseCore 0:
  10.8 115.0 all-gather.11
  128.6 110.4 all-gather.5
  246.5 19.5 all-reduce.2
  268.7 97.1 all-gather.7
  368.4 74.1 all-gather.9
